TPU v7x, 32 devices: a whole 2x2x4 slice. The times are simulated.
32 devices in a mesh: kv: 16 (over z, y, x), tp: 2 (over core).
Axes of the slice: x: 2, y: 2, z: 4, core: 2. Of those that a mesh axis runs over, the one named last changes fastest.
Arguments:
- tokens: bfloat16 [32, 4096], P(None, 'kv'), may hold values from -16 to 16
- mix_gain: bfloat16 [4096], P('kv'), may hold values from 0.099609375 to 1.8984375
- ffn_gain: bfloat16 [4096], P('kv'), may hold values from 0.099609375 to 1.8984375
- w_query: bfloat16 [4096, 2048], P('kv', 'tp'), may hold values from -0.09375 to 0.09375
- w_key: bfloat16 [4096, 2048], P('kv', 'tp'), may hold values from -0.09375 to 0.09375
- w_value: bfloat16 [4096, 4096], P('kv', 'tp'), may hold values from -0.09375 to 0.09375
- w_gate: bfloat16 [4096, 4096], P('kv', 'tp'), may hold values from -0.09375 to 0.09375
- w_decay: bfloat16 [4096, 2048], P('kv', 'tp'), may hold values from -0.375 to 0.375
- decay_bias: float32 [2048], P('tp'), may hold values from -7 to 4
- head_gain: bfloat16 [512], replicated, may hold values from 0.099609375 to 1.8984375
- w_output: bfloat16 [4096, 4096], P('tp', 'kv'), may hold values from -0.09375 to 0.09375
- w_ffgate: bfloat16 [4096, 11008], P('kv', 'tp'), may hold values from -0.09375 to 0.09375
- w_ffup: bfloat16 [4096, 11008], P('kv', 'tp'), may hold values from -0.09375 to 0.09375
- w_down: bfloat16 [11008, 4096], P('tp', 'kv'), may hold values from -0.0546875 to 0.0546875
- state: float32 [32, 8, 256, 512], P('kv', 'tp'), may hold values from -6 to 6
Outputs:
- mixed: bfloat16 [32, 4096], P(None, 'kv')
- new_state: float32 [32, 8, 256, 512], P('kv', 'tp')
All inputs are finite; a program needn't handle non-finite values.
Results may differ from a plain program's by a relative error of at most 0.015.
Values may be sent and summed in bfloat16 or wider, within the bound.
A program may use at most 64 MiB of HBM per device.

v0:
```python
import jax
import jax.numpy as jnp
from jax import lax
from jax.sharding import PartitionSpec as P

epsilon = 1e-06


def local(
    tokens,
    mix_gain,
    ffn_gain,
    w_query,
    w_key,
    w_value,
    w_gate,
    w_decay,
    decay_bias,
    head_gain,
    w_output,
    w_ffgate,
    w_ffup,
    w_down,
    state,
):
    own_rows = state.shape[0]
    local_heads = state.shape[1]
    key_dim = state.shape[2]
    val_dim = state.shape[3]
    model_width = tokens.shape[1] * lax.axis_size("kv")
    row_offset = lax.axis_index("kv") * own_rows
    token_f32 = tokens.astype(jnp.float32)
    row_squares = jnp.sum(token_f32 * token_f32, axis=1)
    mix_in = (token_f32 * mix_gain.astype(jnp.float32)).astype(jnp.bfloat16)
    query_part = jnp.dot(mix_in, w_query, preferred_element_type=jnp.float32)
    key_part = jnp.dot(mix_in, w_key, preferred_element_type=jnp.float32)
    value_part = jnp.dot(mix_in, w_value, preferred_element_type=jnp.float32)
    gate_part = jnp.dot(mix_in, w_gate, preferred_element_type=jnp.float32)
    decay_part = jnp.dot(mix_in, w_decay, preferred_element_type=jnp.float32)
    square_total = lax.psum(row_squares, "kv")
    own_squares = lax.dynamic_slice_in_dim(square_total, row_offset, own_rows)
    query_sum, key_sum, value_sum, gate_sum, decay_sum = (
        lax.psum_scatter(query_part, "kv", scatter_dimension=0, tiled=True),
        lax.psum_scatter(key_part, "kv", scatter_dimension=0, tiled=True),
        lax.psum_scatter(value_part, "kv", scatter_dimension=0, tiled=True),
        lax.psum_scatter(gate_part, "kv", scatter_dimension=0, tiled=True),
        lax.psum_scatter(decay_part, "kv", scatter_dimension=0, tiled=True),
    )
    mix_rms = lax.rsqrt(own_squares / model_width + epsilon)[:, None]
    queries = (query_sum * mix_rms).reshape(own_rows, local_heads, key_dim) * key_dim ** (-0.5)
    key_rows = (key_sum * mix_rms).reshape(own_rows, local_heads, key_dim)
    value_rows = (value_sum * mix_rms).reshape(own_rows, local_heads, val_dim)
    gate_rows = (gate_sum * mix_rms).reshape(own_rows, local_heads, val_dim)
    decay_rows = (decay_sum * mix_rms + decay_bias).reshape(own_rows, local_heads, key_dim)
    log_decay = jax.nn.log_sigmoid(decay_rows) / 16.0
    new_state = (
        jnp.exp(log_decay)[..., None] * state + key_rows[..., :, None] * value_rows[..., None, :]
    )
    attended = jnp.einsum("bhk,bhkv->bhv", queries, new_state, precision=lax.Precision.HIGHEST)
    attended = attended * lax.rsqrt(
        jnp.sum(attended * attended, axis=2, keepdims=True) / val_dim + epsilon
    )
    head_out = (
        (attended * head_gain.astype(jnp.float32) * jax.nn.silu(gate_rows))
        .reshape(own_rows, local_heads * val_dim)
        .astype(jnp.bfloat16)
    )
    head_partial = jnp.dot(
        lax.all_gather(head_out, "kv", axis=0, tiled=True),
        w_output,
        preferred_element_type=jnp.float32,
    )
    attn_out = lax.psum(head_partial.astype(jnp.bfloat16), "tp").astype(jnp.float32)
    residual_mid = (token_f32 + attn_out).astype(jnp.bfloat16)
    mid_f32 = residual_mid.astype(jnp.float32)
    mid_squares = jnp.sum(mid_f32 * mid_f32, axis=1)
    ffn_in = (mid_f32 * ffn_gain.astype(jnp.float32)).astype(jnp.bfloat16)
    ffgate_part = jnp.dot(ffn_in, w_ffgate, preferred_element_type=jnp.float32)
    ffup_part = jnp.dot(ffn_in, w_ffup, preferred_element_type=jnp.float32)
    ffgate_sum, ffup_sum, square_sum = lax.psum((ffgate_part, ffup_part, mid_squares), "kv")
    ffn_rms = lax.rsqrt(square_sum / model_width + epsilon)[:, None]
    hidden = (jax.nn.silu(ffgate_sum * ffn_rms) * (ffup_sum * ffn_rms)).astype(jnp.bfloat16)
    down_part = jnp.dot(hidden, w_down, preferred_element_type=jnp.float32)
    ffn_out = lax.psum(down_part.astype(jnp.bfloat16), "tp").astype(jnp.float32)
    mixed = (mid_f32 + ffn_out).astype(jnp.bfloat16)
    return (mixed, new_state)


def solution(mesh):
    in_specs = (
        P(None, "kv"),
        P("kv"),
        P("kv"),
        P("kv", "tp"),
        P("kv", "tp"),
        P("kv", "tp"),
        P("kv", "tp"),
        P("kv", "tp"),
        P("tp"),
        P(),
        P("tp", "kv"),
        P("kv", "tp"),
        P("kv", "tp"),
        P("tp", "kv"),
        P("kv", "tp", None, None),
    )
    out_specs = (P(None, "kv"), P("kv", "tp", None, None))
    return jax.shard_map(local, mesh=mesh, in_specs=in_specs, out_specs=out_specs, check_vma=False)
```

profile of v0, /device:TPU:1, one launch (start us, length us, event | category | flops | bytes accessed | tf_op | source)
XLA Modules:
  0.0 317.4 jit_solution(6141432531111428591)
XLA Ops:
  7.2 0.0 copy-start
  7.2 0.0 copy-start.7
  7.2 0.0 copy-start.3
  7.2 0.0 copy-start.6
  7.2 0.0 copy-start.5
  7.2 0.0 copy-start.4
  7.2 0.0 all-reduce.12.cloned.1.call-start
  7.3 0.8 convert_element_type.49
  8.1 1.9 fusion.28
  10.0 1.9 fusion.26
  11.9 1.9 fusion.30
  13.9 2.2 fusion.24
  16.1 2.2 fusion.22
  18.3 0.0 all-reduce.12.cloned.1.call-update
  18.3 0.0 all-reduce.10.cloned.1.call-start
  18.4 0.0 copy-done.6
  18.4 0.0 copy-done.5
  18.5 0.0 copy-done.7
  18.5 0.6 dynamic-slice
  19.7 0.0 copy-done.3
  19.7 0.1 fusion.3
  19.8 36.2 %psum.42 = f32[32]{0:T(128)S(1)} all-reduce(f32[32]{0:T(128)S(1)} %fusion.3), channel_id=1, replica_groups=mesh['kv'=16,'tp'=2] {'kv'}, use_global_device_ids=true, to_apply=%region_2.0 | all-reduce | flops 32 | bytes 256 | tf_op jit(solution)/shard_map/psum | solution.py:40
  56.0 0.1 add_rsqrt_fusion.2
  56.1 75.9 %all-reduce.12.cloned.1.call-done = (f32[32,2048]{1,0:T(8,128)}, f32[32,1024]{1,0:T(8,128)}, f32[32,2048]{1,0:T(8,128)}, f32[32,1024]{1,0:T(8,128)}, f32[32,1024]{1,0:T(8,128)}) async-done(((f32[32,2048]{1,0:T(8,128)}, f32[32,1024]{1,0:T(8,128)}, f32[32,2048]{1,0:T(8,128)}, f32[32,1024]{1,0:T(8,128)}, f32[32,1024]{1,0:T(8,128)}), (f32[32,2048]{1,0:T(8,128)}, f32[32,1024]{1,0:T(8,128)}, ...) | async-done | bytes 917520
  132.0 0.0 copy-done.4
  132.0 0.9 fusion.20
  132.9 1.0 dynamic-slice_multiply_fusion.1
  134.0 2.6 multiply_add_fusion
  136.6 0.0 copy-start.1
  136.6 2.0 copy-done.1
  138.6 2.1 fusion.34
  140.7 0.1 fusion.9
  140.8 0.1 fusion.11
  140.9 33.1 %all-gather = bf16[16,2,2048]{2,1,0:T(2,128)(2,1)S(1)} all-gather(bf16[1,2,2048]{2,1,0:T(2,128)(2,1)S(1)} %reshape.47), channel_id=1, replica_groups=mesh['kv'=16,'tp'=2] {'kv'}, dimensions={0}, use_global_device_ids=true | all-gather | bytes 139264 | tf_op jit(solution)/shard_map/all_gather | solution.py:69
  174.0 0.1 reshape.48
  174.1 1.5 convolution_convert_fusion.1
  175.6 12.1 %psum.43 = bf16[32,256]{1,0:T(8,128)(2,1)S(1)} all-reduce(bf16[32,256]{1,0:T(8,128)(2,1)S(1)} %convolution_convert_fusion.1), channel_id=1, replica_groups=mesh['kv'=16,'tp'=2] {'tp'}, use_global_device_ids=true, to_apply=%region_8.9 | all-reduce | flops 8192 | bytes 32768 | tf_op jit(solution)/shard_map/psum | solution.py:73
  187.6 0.0 copy-start.2
  187.6 0.1 fusion.6
  187.8 0.0 copy-done
  187.8 1.5 fusion.12
  189.2 0.5 copy-done.2
  189.7 1.4 fusion.14
  191.1 0.0 all-reduce.10.cloned.1.call-update
  191.2 30.1 %psum.45 = f32[32]{0:T(128)S(1)} all-reduce(f32[32]{0:T(128)S(1)} %get-tuple-element.9), channel_id=1, replica_groups=mesh['kv'=16,'tp'=2] {'kv'}, use_global_device_ids=true, to_apply=%region_11.12 | all-reduce | flops 32 | bytes 256 | tf_op jit(solution)/shard_map/psum | solution.py:80
  221.2 81.3 %all-reduce.10.cloned.1.call-done = (f32[32,5504]{1,0:T(8,128)}, f32[32,5504]{1,0:T(8,128)}) async-done(((f32[32,5504]{1,0:T(8,128)}, f32[32,5504]{1,0:T(8,128)}), (f32[32,5504]{1,0:T(8,128)}, f32[32,5504]{1,0:T(8,128)})) %all-reduce.10.cloned.1.call-update) | async-done | bytes 1409040 | tf_op jit(solution)/shard_map/psum | solution.py:80
  302.6 2.8 convolution_convert_fusion
  305.4 4.5 %psum.47 = bf16[32,256]{1,0:T(8,128)(2,1)S(1)} all-reduce(bf16[32,256]{1,0:T(8,128)(2,1)S(1)} %convolution_convert_fusion), channel_id=1, replica_groups=mesh['kv'=16,'tp'=2] {'tp'}, use_global_device_ids=true, to_apply=%region_13.14 | all-reduce | flops 8192 | bytes 32768 | tf_op jit(solution)/shard_map/psum | solution.py:84
  310.0 0.6 fusion.7
  (11 shorter events, 0.2 us)
Async XLA Ops:
  7.2 180.6 %copy-start = (bf16[256,5504]{1,0:T(8,128)(2,1)S(1)}, bf16[256,5504]{1,0:T(8,128)(2,1)}, u32[]{:S(2)}) copy-start(bf16[256,5504]{1,0:T(8,128)(2,1)} %param.27) | copy-start | bytes 8454148
  7.2 11.3 %copy-start.7 = (u32[32]{0:T(128)S(1)}, u32[32]{0:T(128)}, u32[]{:S(2)}) copy-start(u32[32]{0:T(128)} %constant.41) | copy-start | bytes 388
  7.2 12.5 %copy-start.3 = (bf16[32,256]{1,0:T(8,128)(2,1)S(1)}, bf16[32,256]{1,0:T(8,128)(2,1)}, u32[]{:S(2)}) copy-start(bf16[32,256]{1,0:T(8,128)(2,1)} %param.15) | copy-start | bytes 49156
  7.2 11.2 %copy-start.6 = (bf16[256]{0:T(256)(128)(2,1)S(1)}, bf16[256]{0:T(256)(128)(2,1)}, u32[]{:S(2)}) copy-start(bf16[256]{0:T(256)(128)(2,1)} %param.17) | copy-start | bytes 1540
  7.2 11.2 %copy-start.5 = (bf16[512]{0:T(512)(128)(2,1)S(1)}, bf16[512]{0:T(512)(128)(2,1)}, u32[]{:S(2)}) copy-start(bf16[512]{0:T(512)(128)(2,1)} %param.24) | copy-start | bytes 3076
  7.2 124.8 %copy-start.4 = (f32[1024]{0:T(1024)S(1)}, f32[1024]{0:T(1024)}, u32[]{:S(2)}) copy-start(f32[1024]{0:T(1024)} %param.23) | copy-start | bytes 12292
  7.2 124.7 %all-reduce.12.cloned.1.call-start = ((), (), s32[]{:S(2)}) async-start(), calls=%async_computation.1 | async-start | bytes 1835008
  18.3 284.2 %all-reduce.10.cloned.1.call-start = ((), (), s32[]{:S(2)}) async-start(), calls=%async_computation | async-start | bytes 2818048 | tf_op jit(solution)/shard_map/psum | solution.py:80
  136.6 2.0 copy-start.1
  187.6 2.1 copy-start.2
Sparse Core Ops, SparseCore 0:
  18.5 113.4 all-reduce.11
  191.3 111.2 all-reduce.9
where the time goes:
time: 318 us; the launch traced here: 317 us
  waiting for transfers between devices  157 us (49%)
  blocking collectives  116 us (36%)
  matrix products  19.6 us (6%)
  between operations  14.9 us (5%)
  other arithmetic  6.38 us (2%)
  local copies, waits for them, and re-layouts  3.26 us (1%)
    psum x1, waiting for transfers between devices, local(): lax.psum((ffgate_part, ffup_part, mid_squares), 'kv')  81.3 us
    unnamed x3, waiting for transfers between devices  75.9 us
    psum x1, blocking collectives, local(): square_total = lax.psum(row_squares, 'kv')  36.2 us
    all_gather x1, blocking collectives, local(): lax.all_gather(head_out, 'kv', axis=0, tiled=True)  33.1 us
    psum x1, blocking collectives, local(): lax.psum((ffgate_part, ffup_part, mid_squares), 'kv')  30.1 us
    psum x1, blocking collectives, local(): lax.psum(head_partial.astype(jnp.bfloat16), 'tp').astype(jnp.float32)  12.1 us
  transfers between devices with their start and end apart: 2, of which 2 were waited for; matrix products, arithmetic and copies ran while one was open for 0% of the time, Pallas kernels for 0%

commit v1 on v0

--- a/solution.py
+++ b/solution.py
@@ -1,12 +1,424 @@
+import functools
+
 import jax
 import jax.numpy as jnp
+import numpy as np
 from jax import lax
+from jax.experimental import pallas as pl
+from jax.experimental.pallas import tpu as pltpu
 from jax.sharding import PartitionSpec as P
 
 epsilon = 1e-06
-
-
-def local(
+MESH = pl.DeviceIdType.MESH
+LANES = 128
+FF_CHUNKS = 4
+f32 = jnp.float32
+bf16 = jnp.bfloat16
+
+
+def split_kv(count):
+    near = next(n for n in range(1, count + 1) if count % n == 0 and n * n >= count)
+    return near, count // near
+
+
+def ff_bounds(units):
+    tiles = units // LANES
+    cuts = [(tiles * step + FF_CHUNKS // 2) // FF_CHUNKS * LANES for step in range(FF_CHUNKS + 1)]
+    return list(zip(cuts[:-1], cuts[1:]))
+
+
+def halves(total):
+    high = total.astype(bf16)
+    low = (total - high.astype(f32)).astype(bf16)
+    wide = (total.shape[0], LANES)
+    return jnp.concatenate(
+        [jnp.broadcast_to(high.astype(f32), wide), jnp.broadcast_to(low.astype(f32), wide)], axis=1
+    )
+
+
+def joined(block):
+    return block[:, 0:1] + block[:, LANES : LANES + 1]
+
+
+def layer_kernel(cfg, *refs):
+    near_n, far_n, own, heads, key_dim, val_dim, model_width = cfg["sizes"]
+    ins, outs, scratch = refs[:14], refs[14:18], list(refs[18:])
+    tokens, params, perm, unperm, w_query, w_key, w_value, w_gate, w_decay = ins[:9]
+    w_output, w_ffgate, w_ffup, w_down, state = ins[9:]
+    mixed_ref, dec_out, key_out, val_out = outs
+
+    def take(count):
+        taken = scratch[:count]
+        del scratch[:count]
+        return taken
+
+    held = take(10)
+    rs_widths, ag_widths = cfg["rs_widths"], cfg["ag_widths"]
+    near_out, near_in = take(len(rs_widths)), take(len(rs_widths))
+    far_out, far_in = take(len(rs_widths)), take(len(rs_widths))
+    ag_far, ag_near = take(len(ag_widths)), take(len(ag_widths))
+    stage = take(1)[0]
+    swap_out, swap_in = take(2)
+    q8, d8, k8, v8, g8, a8 = take(6)
+    load_sem, ns_sem, nr_sem, fs_sem, fr_sem = take(5)
+    gfs_sem, gfr_sem, gns_sem, gnr_sem, ws_sem, wr_sem = take(6)
+
+    kv = lax.axis_index("kv")
+    tp = lax.axis_index("tp")
+    near = lax.rem(kv, near_n)
+    far = lax.div(kv, near_n)
+    block = far_n * own
+    rows = near_n * block
+    width = tokens.shape[1]
+
+    weights = [w_query, w_decay, w_key, w_value, w_gate, state, w_output, w_ffgate, w_ffup, w_down]
+    loads = []
+    for index, (source, target) in enumerate(zip(weights, held)):
+        load = pltpu.make_async_copy(source, target, load_sem.at[index])
+        load.start()
+        loads.append(load)
+    h_query, h_decay, h_key, h_value, h_gate, h_state, h_output, h_ffgate, h_ffup, h_down = held
+
+    def near_peer(step):
+        other = lax.rem(near + step, near_n)
+        return other, {"kv": far * near_n + other}
+
+    def far_peer(step):
+        other = lax.rem(far + step, far_n)
+        return other, {"kv": other * near_n + near}
+
+    barrier = pltpu.get_barrier_semaphore()
+    for step in range(1, near_n):
+        pl.semaphore_signal(barrier, inc=1, device_id=near_peer(step)[1], device_id_type=MESH)
+    for step in range(1, far_n):
+        pl.semaphore_signal(barrier, inc=1, device_id=far_peer(step)[1], device_id_type=MESH)
+    pl.semaphore_signal(barrier, inc=1, device_id={"tp": 1 - tp}, device_id_type=MESH)
+
+    sent = []
+
+    def send(source, target, send_sem, recv_sem, device):
+        copy = pltpu.make_async_remote_copy(
+            src_ref=source,
+            dst_ref=target,
+            send_sem=send_sem,
+            recv_sem=recv_sem,
+            device_id=device,
+            device_id_type=MESH,
+        )
+        copy.start()
+        sent.append(copy)
+
+    def arrived(source, target, send_sem, recv_sem, device):
+        pltpu.make_async_remote_copy(
+            src_ref=source,
+            dst_ref=target,
+            send_sem=send_sem,
+            recv_sem=recv_sem,
+            device_id=device,
+            device_id_type=MESH,
+        ).wait_recv()
+
+    def put_near(ch, first, value):
+        last = first + value.shape[1]
+        for other in range(near_n):
+            near_out[ch][other, :, first:last] = value[other * block : (other + 1) * block].astype(bf16)
+
+    def start_near(ch):
+        for step in range(1, near_n):
+            other, device = near_peer(step)
+            send(near_out[ch].at[other], near_in[ch].at[near], ns_sem.at[ch, step], nr_sem.at[ch, step], device)
+
+    def sum_near(ch):
+        total = near_out[ch][near].astype(f32)
+        for step in range(1, near_n):
+            origin = lax.rem(near + near_n - step, near_n)
+            arrived(
+                near_out[ch].at[origin],
+                near_in[ch].at[origin],
+                ns_sem.at[ch, step],
+                nr_sem.at[ch, step],
+                {"kv": far * near_n + origin},
+            )
+            total = total + near_in[ch][origin].astype(f32)
+        return total
+
+    def to_far(ch, squares_at=None):
+        total = sum_near(ch)
+        for other in range(far_n):
+            piece = total[other * own : (other + 1) * own]
+            if squares_at is None:
+                far_out[ch][other] = piece.astype(bf16)
+            else:
+                far_out[ch][other, :, :squares_at] = piece[:, :squares_at].astype(bf16)
+                far_out[ch][other, :, squares_at:] = halves(joined(piece[:, squares_at:])).astype(bf16)
+        for step in range(1, far_n):
+            other, device = far_peer(step)
+            send(far_out[ch].at[other], far_in[ch].at[far], fs_sem.at[ch, step], fr_sem.at[ch, step], device)
+
+    def sum_far(ch):
+        total = far_out[ch][far].astype(f32)
+        for step in range(1, far_n):
+            origin = lax.rem(far + far_n - step, far_n)
+            arrived(
+                far_out[ch].at[origin],
+                far_in[ch].at[origin],
+                fs_sem.at[ch, step],
+                fr_sem.at[ch, step],
+                {"kv": origin * near_n + near},
+            )
+            total = total + far_in[ch][origin].astype(f32)
+        return total
+
+    def start_gather(ch):
+        for step in range(1, far_n):
+            _, device = far_peer(step)
+            send(ag_far[ch].at[far], ag_far[ch].at[far], gfs_sem.at[ch, step], gfr_sem.at[ch, step], device)
+
+    def pass_gather(ch):
+        for step in range(1, far_n):
+            origin = lax.rem(far + far_n - step, far_n)
+            arrived(
+                ag_far[ch].at[origin],
+                ag_far[ch].at[origin],
+                gfs_sem.at[ch, step],
+                gfr_sem.at[ch, step],
+                {"kv": origin * near_n + near},
+            )
+        wide = ag_widths[ch]
+        for other in range(far_n):
+            stage[other * own : (other + 1) * own, :wide] = ag_far[ch][other].astype(f32)
+        ag_near[ch][near] = stage[:, :wide].astype(bf16)
+        for step in range(1, near_n):
+            _, device = near_peer(step)
+            send(ag_near[ch].at[near], ag_near[ch].at[near], gns_sem.at[ch, step], gnr_sem.at[ch, step], device)
+
+    def gathered(ch):
+        for step in range(1, near_n):
+            origin = lax.rem(near + near_n - step, near_n)
+            arrived(
+                ag_near[ch].at[origin],
+                ag_near[ch].at[origin],
+                gns_sem.at[ch, step],
+                gnr_sem.at[ch, step],
+                {"kv": far * near_n + origin},
+            )
+        return jnp.concatenate([ag_near[ch][other].astype(f32) for other in range(near_n)], axis=0).astype(bf16)
+
+    def over_groups(use, partial):
+        swap_out[use] = partial.astype(bf16)
+        send(swap_out.at[use], swap_in.at[use], ws_sem.at[use], wr_sem.at[use], {"tp": 1 - tp})
+        arrived(swap_out.at[use], swap_in.at[use], ws_sem.at[use], wr_sem.at[use], {"tp": 1 - tp})
+        return swap_out[use].astype(f32) + swap_in[use].astype(f32)
+
+    mix_gain = params[:, :width]
+    ffn_gain = params[:, width : 2 * width]
+    head_gain = params[:, 2 * width : 2 * width + val_dim]
+    decay_bias = params[:, 2 * width + val_dim :]
+
+    token_f32 = jnp.dot(perm[...], tokens[...], preferred_element_type=f32)
+    mix_in = (token_f32 * mix_gain).astype(bf16)
+    attn_channels = ((0, h_query, 0), (1, h_decay, 1), (2, h_key, 2), (3, h_value, 3), (4, h_gate, 4))
+    for ch, weight, load in attn_channels:
+        loads[load].wait()
+        put_near(ch, 0, jnp.dot(mix_in, weight[...], preferred_element_type=f32))
+        if ch == 0:
+            squares = jnp.sum(token_f32 * token_f32, axis=1, keepdims=True)
+            put_near(0, weight.shape[1], halves(squares))
+            pl.semaphore_wait(barrier, near_n + far_n - 1)
+        start_near(ch)
+    key_cols = heads * key_dim
+    for ch in range(5):
+        to_far(ch, key_cols if ch == 0 else None)
+
+    def by_head(target, wide, value):
+        for row in range(own):
+            for head in range(heads):
+                slot = row * heads + head
+                target[slot : slot + 1, :] = value[row : row + 1, head * wide : (head + 1) * wide]
+
+    total = sum_far(0)
+    mix_rms = lax.rsqrt(joined(total[:, key_cols:]) / model_width + epsilon)
+    by_head(q8, key_dim, total[:, :key_cols] * mix_rms * key_dim ** (-0.5))
+    by_head(d8, key_dim, sum_far(1) * mix_rms + decay_bias)
+    decay_in = d8[...]
+    log_decay = (jnp.minimum(decay_in, 0.0) - jnp.log1p(jnp.exp(-jnp.abs(decay_in)))) / 16.0
+    decay = jnp.exp(log_decay)
+    dec_out[...] = decay.T
+    scaled = (q8[...] * decay).T
+    loads[5].wait()
+    for row in range(own):
+        for head in range(heads):
+            slot = row * heads + head
+            a8[slot : slot + 1, :] = jnp.sum(h_state[row, head] * scaled[:, slot : slot + 1], axis=0, keepdims=True)
+    by_head(k8, key_dim, sum_far(2) * mix_rms)
+    key_out[...] = k8[...].T
+    by_head(v8, val_dim, sum_far(3) * mix_rms)
+    val_out[...] = v8[...]
+    by_head(g8, val_dim, sum_far(4) * mix_rms)
+    attended = a8[...] + jnp.sum(q8[...] * k8[...], axis=1, keepdims=True) * v8[...]
+    attended = attended * lax.rsqrt(jnp.sum(attended * attended, axis=1, keepdims=True) / val_dim + epsilon)
+    gates = g8[...]
+    a8[...] = attended * head_gain * (gates / (1.0 + jnp.exp(-gates)))
+    for row in range(own):
+        for head in range(heads):
+            slot = row * heads + head
+            stage[row : row + 1, head * val_dim : (head + 1) * val_dim] = a8[slot : slot + 1, :]
+    ag_far[0][far] = stage[:own, : heads * val_dim].astype(bf16)
+    start_gather(0)
+    pass_gather(0)
+    loads[6].wait()
+    head_partial = jnp.dot(gathered(0), h_output[...], preferred_element_type=f32)
+    residual_mid = (token_f32 + over_groups(0, head_partial)).astype(bf16)
+
+    mid_f32 = residual_mid.astype(f32)
+    ffn_in = (mid_f32 * ffn_gain).astype(bf16)
+    bounds = cfg["bounds"]
+    loads[7].wait()
+    loads[8].wait()
+    for index, (low, high) in enumerate(bounds):
+        ch = 5 + index
+        put_near(ch, 0, jnp.dot(ffn_in, h_ffgate[:, low:high], preferred_element_type=f32))
+        put_near(ch, high - low, jnp.dot(ffn_in, h_ffup[:, low:high], preferred_element_type=f32))
+        if index == 0:
+            put_near(ch, 2 * (high - low), halves(jnp.sum(mid_f32 * mid_f32, axis=1, keepdims=True)))
+        start_near(ch)
+    loads[9].wait()
+
+    ffn_rms = None
+    down = jnp.zeros((rows, width), f32)
+    for turn in range(len(bounds) + 3):
+        if turn < len(bounds):
+            low, high = bounds[turn]
+            to_far(5 + turn, 2 * (high - low) if turn == 0 else None)
+        index = turn - 1
+        if 0 <= index < len(bounds):
+            wide = bounds[index][1] - bounds[index][0]
+            total = sum_far(5 + index)
+            if index == 0:
+                ffn_rms = lax.rsqrt(joined(total[:, 2 * wide :]) / model_width + epsilon)
+            gate = total[:, :wide] * ffn_rms
+            up = total[:, wide : 2 * wide] * ffn_rms
+            ag_far[1 + index][far] = (gate / (1.0 + jnp.exp(-gate)) * up).astype(bf16)
+            start_gather(1 + index)
+        index = turn - 2
+        if 0 <= index < len(bounds):
+            pass_gather(1 + index)
+        index = turn - 3
+        if 0 <= index < len(bounds):
+            low, high = bounds[index]
+            down = down + jnp.dot(gathered(1 + index), h_down[low:high, :], preferred_element_type=f32)
+    mixed = (mid_f32 + over_groups(1, down)).astype(bf16)
+    mixed_ref[...] = jnp.dot(unperm[...], mixed, preferred_element_type=f32).astype(bf16)
+    for copy in sent:
+        copy.wait_send()
+
+
+def state_kernel(decay, keys, values, state, new_state):
+    heads = pl.num_programs(1)
+    slot = pl.program_id(0) * heads + pl.program_id(1)
+    chosen = lax.broadcasted_iota(jnp.int32, decay.shape, 1) == slot
+    decay_col = jnp.sum(jnp.where(chosen, decay[...], 0.0), axis=1, keepdims=True)
+    key_col = jnp.sum(jnp.where(chosen, keys[...], 0.0), axis=1, keepdims=True)
+    new_state[0, 0] = decay_col * state[0, 0] + key_col * values[pl.ds(slot, 1), :]
+
+
+def local_fused(
+    tokens,
+    mix_gain,
+    ffn_gain,
+    w_query,
+    w_key,
+    w_value,
+    w_gate,
+    w_decay,
+    decay_bias,
+    head_gain,
+    w_output,
+    w_ffgate,
+    w_ffup,
+    w_down,
+    state,
+):
+    own, heads, key_dim, val_dim = state.shape
+    rows, width = tokens.shape
+    kv_n = lax.axis_size("kv")
+    near_n, far_n = split_kv(kv_n)
+    block = far_n * own
+    slots = own * heads
+    bounds = ff_bounds(w_down.shape[0])
+    key_cols, val_cols = heads * key_dim, heads * val_dim
+    rs_widths = [key_cols + 2 * LANES, key_cols, key_cols, val_cols, val_cols]
+    rs_widths += [2 * (high - low) + (2 * LANES if low == 0 else 0) for low, high in bounds]
+    ag_widths = [val_cols] + [high - low for low, high in bounds]
+    cfg = {
+        "sizes": (near_n, far_n, own, heads, key_dim, val_dim, width * kv_n),
+        "rs_widths": rs_widths,
+        "ag_widths": ag_widths,
+        "bounds": bounds,
+    }
+    origin = np.arange(rows).reshape(far_n, near_n, own).transpose(1, 0, 2).reshape(-1)
+    order = np.zeros((rows, rows), np.float32)
+    order[np.arange(rows), origin] = 1.0
+    params = jnp.concatenate([mix_gain.astype(f32), ffn_gain.astype(f32), head_gain.astype(f32), decay_bias])[None]
+    held = [w_query, w_decay, w_key, w_value, w_gate, state, w_output, w_ffgate, w_ffup, w_down]
+    scratch = [pltpu.VMEM(array.shape, array.dtype) for array in held]
+    scratch += [pltpu.VMEM((near_n, block, wide), bf16) for wide in rs_widths] * 2
+    scratch += [pltpu.VMEM((far_n, own, wide), bf16) for wide in rs_widths] * 2
+    scratch += [pltpu.VMEM((far_n, own, wide), bf16) for wide in ag_widths]
+    scratch += [pltpu.VMEM((near_n, block, wide), bf16) for wide in ag_widths]
+    scratch += [pltpu.VMEM((block, max(ag_widths)), f32)]
+    scratch += [pltpu.VMEM((2, rows, width), bf16)] * 2
+    scratch += [pltpu.VMEM((slots, wide), f32) for wide in (key_dim, key_dim, key_dim, val_dim, val_dim, val_dim)]
+    dma = pltpu.SemaphoreType.DMA
+    scratch += [dma((len(held),))]
+    scratch += [dma((len(rs_widths), near_n))] * 2 + [dma((len(rs_widths), far_n))] * 2
+    scratch += [dma((len(ag_widths), far_n))] * 2 + [dma((len(ag_widths), near_n))] * 2
+    scratch += [dma((2,))] * 2
+    vmem = pl.BlockSpec(memory_space=pltpu.VMEM)
+    hbm = pl.BlockSpec(memory_space=pl.ANY)
+    mixed, decay, keys, values = pl.pallas_call(
+        functools.partial(layer_kernel, cfg),
+        out_shape=(
+            jax.ShapeDtypeStruct((rows, width), bf16),
+            jax.ShapeDtypeStruct((key_dim, slots), f32),
+            jax.ShapeDtypeStruct((key_dim, slots), f32),
+            jax.ShapeDtypeStruct((slots, val_dim), f32),
+        ),
+        in_specs=[vmem] * 4 + [hbm] * 10,
+        out_specs=(vmem,) * 4,
+        scratch_shapes=scratch,
+        compiler_params=pltpu.CompilerParams(
+            collective_id=0, has_side_effects=True, vmem_limit_bytes=48 * 1024 * 1024
+        ),
+    )(
+        tokens,
+        params,
+        jnp.asarray(order, bf16),
+        jnp.asarray(order.T, bf16),
+        w_query,
+        w_key,
+        w_value,
+        w_gate,
+        w_decay,
+        w_output,
+        w_ffgate,
+        w_ffup,
+        w_down,
+        state,
+    )
+    whole = pl.BlockSpec((key_dim, slots), lambda row, head: (0, 0))
+    tile = pl.BlockSpec((1, 1, key_dim, val_dim), lambda row, head: (row, head, 0, 0))
+    new_state = pl.pallas_call(
+        state_kernel,
+        grid=(own, heads),
+        out_shape=jax.ShapeDtypeStruct(state.shape, f32),
+        in_specs=[whole, whole, pl.BlockSpec((slots, val_dim), lambda row, head: (0, 0)), tile],
+        out_specs=tile,
+    )(decay, keys, values, state)
+    return (mixed, new_state)
+
+
+def local_plain(
     tokens,
     mix_gain,
     ffn_gain,
@@ -86,6 +498,27 @@
     return (mixed, new_state)
 
 
+def fits(tokens, w_query, w_down, state):
+    own, heads, key_dim, val_dim = state.shape
+    near_n, far_n = split_kv(lax.axis_size("kv"))
+    return (
+        lax.axis_size("tp") == 2
+        and near_n > 1
+        and far_n > 1
+        and (far_n * own) % 8 == 0
+        and (own * heads) % 8 == 0
+        and all(extent % LANES == 0 for extent in (tokens.shape[1], key_dim, val_dim, w_down.shape[0]))
+        and w_down.shape[0] // LANES >= FF_CHUNKS
+    )
+
+
+def local(*arrays):
+    tokens, w_query, w_down, state = arrays[0], arrays[3], arrays[13], arrays[14]
+    if fits(tokens, w_query, w_down, state):
+        return local_fused(*arrays)
+    return local_plain(*arrays)
+
+
 def solution(mesh):
     in_specs = (
         P(None, "kv"),

time: 318 us -> 73.2 us (0.23)
  waiting for transfers between devices: 157 us -> 0 us
  blocking collectives: 116 us -> 0 us
  Pallas kernels: 0 us -> 58.5 us
  matrix products: 19.6 us -> 0 us
  between operations: 14.9 us -> 0.66 us
  local copies, waits for them, and re-layouts: 3.26 us -> 10.7 us
  other arithmetic: 6.38 us -> 2.69 us
    psum x4 -> x0, blocking collectives: 82.9 us -> none  [the longest x1 36.2 us: local(): square_total = lax.psum(row_squares, 'kv')]
    psum x1 -> x0, waiting for transfers between devices: 81.3 us -> none  [local(): lax.psum((ffgate_part, ffup_part, mid_squares), 'kv')]
    unnamed x3 -> x0, waiting for transfers between devices: 75.9 us -> none
    pallas_call x0 -> x2, Pallas kernels: none -> 58.5 us  [the longest x1 51.3 us: local_fused(): pl.pallas_call(functools.partial(layer_kernel, cfg), out_shape=(jax.Shape...]
    all_gather x1 -> x0, blocking collectives: 33.1 us -> none  [local(): lax.all_gather(head_out, 'kv', axis=0, tiled=True)]
    dot_general x10 -> x0, matrix products: 19.6 us -> none  [the longest x1 2.83 us: local(): down_part = jnp.dot(hidden, w_down, preferred_element_type=jnp.float32)]
    unnamed x19 -> x23, local copies, waits for them, and re-layouts: 3.15 us -> 10.7 us
  transfers between devices with their start and end apart: 2 -> 0, of which waited for: 2 -> 0; matrix products, arithmetic and copies ran while one was open for 0% -> 0% of each run, Pallas kernels for 0% -> 0%
where the time goes in v1:
time: 73.2 us; the launch traced here: 72.5 us
  Pallas kernels  58.5 us (80%)
  local copies, waits for them, and re-layouts  10.7 us (15%)
  other arithmetic  2.69 us (4%)
    pallas_call x1, Pallas kernels, local_fused(): pl.pallas_call(functools.partial(layer_kernel, cfg), out_shape=(jax.Shape...  51.3 us
    unnamed x23, local copies, waits for them, and re-layouts  10.7 us
    pallas_call x1, Pallas kernels, local_fused(): pl.pallas_call(state_kernel, grid=(own, heads), out_shape=jax.ShapeDtypeS...  7.12 us

profile of v1, /device:TPU:1, one launch (start us, length us, event | category | flops | bytes accessed | tf_op | source)
XLA Modules:
  0.0 72.5 jit_solution(7737720795740792519)
XLA Ops:
  0.6 0.7 convert_element_type.9
  1.3 0.7 convert_element_type.10
  1.9 0.7 convert_element_type.11
  2.6 0.7 pad_maximum_fusion
  3.3 0.0 copy-start
  3.3 1.2 %copy-done = bf16[256,2048]{1,0:T(8,128)(2,1)S(1)} copy-done((bf16[256,2048]{1,0:T(8,128)(2,1)S(1)}, bf16[256,2048]{1,0:T(8,128)(2,1)}, u32[]{:S(2)}) %copy-start) | copy-done | bytes 1048600
  4.5 0.0 copy-start.1
  4.5 1.2 %copy-done.1 = bf16[256,2048]{1,0:T(8,128)(2,1)S(1)} copy-done((bf16[256,2048]{1,0:T(8,128)(2,1)S(1)}, bf16[256,2048]{1,0:T(8,128)(2,1)}, u32[]{:S(2)}) %copy-start.1) | copy-done | bytes 1048600
  5.8 0.0 copy-start.2
  5.8 1.2 %copy-done.2 = bf16[2048,256]{1,0:T(8,128)(2,1)S(1)} copy-done((bf16[2048,256]{1,0:T(8,128)(2,1)S(1)}, bf16[2048,256]{1,0:T(8,128)(2,1)}, u32[]{:S(2)}) %copy-start.2) | copy-done | bytes 1048600
  7.0 0.0 copy-start.3
  7.0 1.0 %copy-done.3 = bf16[256,1024]{1,0:T(8,128)(2,1)S(1)} copy-done((bf16[256,1024]{1,0:T(8,128)(2,1)S(1)}, bf16[256,1024]{1,0:T(8,128)(2,1)}, u32[]{:S(2)}) %copy-start.3) | copy-done | bytes 524312
  8.0 0.0 copy-start.4
  8.0 1.0 %copy-done.4 = bf16[256,1024]{1,0:T(8,128)(2,1)S(1)} copy-done((bf16[256,1024]{1,0:T(8,128)(2,1)S(1)}, bf16[256,1024]{1,0:T(8,128)(2,1)}, u32[]{:S(2)}) %copy-start.4) | copy-done | bytes 524312
  9.1 0.0 copy-start.5
  9.1 1.0 %copy-done.5 = bf16[256,1024]{1,0:T(8,128)(2,1)S(1)} copy-done((bf16[256,1024]{1,0:T(8,128)(2,1)S(1)}, bf16[256,1024]{1,0:T(8,128)(2,1)}, u32[]{:S(2)}) %copy-start.5) | copy-done | bytes 524312
  10.1 0.0 copy-start.8
  10.1 0.7 copy-done.8
  10.8 0.0 copy-start.10
  10.8 0.7 copy-done.10
  11.5 51.3 %shard_map.176 = (bf16[32,256]{1,0:T(8,128)(2,1)S(1)}, f32[256,8]{1,0:T(8,128)S(1)}, f32[256,8]{1,0:T(8,128)S(1)}, f32[8,512]{1,0:T(8,128)S(1)}) custom-call(bf16[32,256]{1,0:T(8,128)(2,1)S(1)} %copy-done.10, f32[1,2048]{1,0:T(1,128)S(1)} %bitcast.1, bf16[32,32]{1,0:T(8,128)(2,1)S(1)} %copy-done.8, bf16[32,32]{1,0:T(8,128)(2,1)S(1)} %copy-done.8, ...), custom_call_target="tpu_custom_call" | custom-call | tf_op jit(solution)/shard_map/pallas_call | solution.py:379
  62.9 0.0 copy-start.6
  62.9 0.6 copy-done.6
  63.5 0.0 copy-start.7
  63.5 0.7 copy-done.7
  64.2 0.0 copy-start.9
  64.2 0.6 copy-done.9
  64.8 7.1 %shard_map.177 = f32[2,4,256,512]{3,2,1,0:T(8,128)} custom-call(f32[256,8]{1,0:T(8,128)} %copy-done.6, f32[256,8]{1,0:T(8,128)} %copy-done.7, f32[8,512]{1,0:T(8,128)} %copy-done.9, f32[2,4,256,512]{3,2,1,0:T(8,128)} %state.1), custom_call_target="tpu_custom_call" | custom-call | tf_op jit(solution)/shard_map/pallas_call | solution.py:411
  71.9 0.6 copy.20
Async XLA Ops:
  3.3 1.2 %copy-start = (bf16[256,2048]{1,0:T(8,128)(2,1)S(1)}, bf16[256,2048]{1,0:T(8,128)(2,1)}, u32[]{:S(2)}) copy-start(bf16[256,2048]{1,0:T(8,128)(2,1)} %refs_6_.1) | copy-start | bytes 3145732
  4.5 1.2 %copy-start.1 = (bf16[256,2048]{1,0:T(8,128)(2,1)S(1)}, bf16[256,2048]{1,0:T(8,128)(2,1)}, u32[]{:S(2)}) copy-start(bf16[256,2048]{1,0:T(8,128)(2,1)} %refs_7_.1) | copy-start | bytes 3145732
  5.8 1.2 %copy-start.2 = (bf16[2048,256]{1,0:T(8,128)(2,1)S(1)}, bf16[2048,256]{1,0:T(8,128)(2,1)}, u32[]{:S(2)}) copy-start(bf16[2048,256]{1,0:T(8,128)(2,1)} %refs_9_.1) | copy-start | bytes 3145732
  7.0 1.0 %copy-start.3 = (bf16[256,1024]{1,0:T(8,128)(2,1)S(1)}, bf16[256,1024]{1,0:T(8,128)(2,1)}, u32[]{:S(2)}) copy-start(bf16[256,1024]{1,0:T(8,128)(2,1)} %refs_4_.1) | copy-start | bytes 1572868
  8.0 1.0 %copy-start.4 = (bf16[256,1024]{1,0:T(8,128)(2,1)S(1)}, bf16[256,1024]{1,0:T(8,128)(2,1)}, u32[]{:S(2)}) copy-start(bf16[256,1024]{1,0:T(8,128)(2,1)} %refs_5_.1) | copy-start | bytes 1572868
  9.1 1.0 %copy-start.5 = (bf16[256,1024]{1,0:T(8,128)(2,1)S(1)}, bf16[256,1024]{1,0:T(8,128)(2,1)}, u32[]{:S(2)}) copy-start(bf16[256,1024]{1,0:T(8,128)(2,1)} %refs_8_.1) | copy-start | bytes 1572868
  10.1 0.7 copy-start.8
  10.8 0.7 copy-start.10
  62.9 0.6 copy-start.6
  63.5 0.7 copy-start.7
  64.2 0.6 copy-start.9

commit v2 on v1

--- a/solution.py
+++ b/solution.py
@@ -11,7 +11,10 @@
 epsilon = 1e-06
 MESH = pl.DeviceIdType.MESH
 LANES = 128
-FF_CHUNKS = 4
+FF_CHUNKS = 3
+LAGS = (1, 2, 3)
+ATTN_CHANNELS = (("query", "decay", "key"), ("value",), ("gate",))
+VMEM_BYTES = 67043328
 f32 = jnp.float32
 bf16 = jnp.bfloat16
 
@@ -42,17 +45,15 @@
 
 def layer_kernel(cfg, *refs):
     near_n, far_n, own, heads, key_dim, val_dim, model_width = cfg["sizes"]
-    ins, outs, scratch = refs[:14], refs[14:18], list(refs[18:])
-    tokens, params, perm, unperm, w_query, w_key, w_value, w_gate, w_decay = ins[:9]
-    w_output, w_ffgate, w_ffup, w_down, state = ins[9:]
-    mixed_ref, dec_out, key_out, val_out = outs
+    ins, outs, scratch = refs[:15], refs[15:17], list(refs[17:])
+    mixed_ref, new_state = outs
 
     def take(count):
         taken = scratch[:count]
         del scratch[:count]
         return taken
 
-    held = take(10)
+    held = take(15)
     rs_widths, ag_widths = cfg["rs_widths"], cfg["ag_widths"]
     near_out, near_in = take(len(rs_widths)), take(len(rs_widths))
     far_out, far_in = take(len(rs_widths)), take(len(rs_widths))
@@ -60,8 +61,10 @@
     stage = take(1)[0]
     swap_out, swap_in = take(2)
     q8, d8, k8, v8, g8, a8 = take(6)
+    made = take(1)[0]
     load_sem, ns_sem, nr_sem, fs_sem, fr_sem = take(5)
     gfs_sem, gfr_sem, gns_sem, gnr_sem, ws_sem, wr_sem = take(6)
+    out_sem = take(1)[0]
 
     kv = lax.axis_index("kv")
     tp = lax.axis_index("tp")
@@ -69,18 +72,29 @@
     far = lax.div(kv, near_n)
     block = far_n * own
     rows = near_n * block
-    width = tokens.shape[1]
-
-    weights = [w_query, w_decay, w_key, w_value, w_gate, state, w_output, w_ffgate, w_ffup, w_down]
+    width = ins[0].shape[1]
+
     loads = []
-    for index, (source, target) in enumerate(zip(weights, held)):
+    for index, (source, target) in enumerate(zip(ins, held)):
         load = pltpu.make_async_copy(source, target, load_sem.at[index])
         load.start()
         loads.append(load)
-    h_query, h_decay, h_key, h_value, h_gate, h_state, h_output, h_ffgate, h_ffup, h_down = held
+    tokens, mix_ref, h_query, h_decay, h_key, bias_ref, h_value, h_gate = held[:8]
+    h_state, head_ref, ffn_ref, h_output, h_ffgate, h_ffup, h_down = held[8:]
+
+    pair = 2 if near_n % 2 == 0 else 1
+    shifts = [(a, b) for a in range(pair) for b in range(near_n // pair)]
+    shifts.sort(key=lambda shift: (shift != (0, 0), -(shift[0] > 0) - (shift[1] > 0)))
+
+    def near_shift(step, back=1):
+        a, b = shifts[step]
+        deep = near_n // pair
+        low = lax.rem(lax.rem(near, pair) + pair + back * a, pair)
+        high = lax.rem(lax.div(near, pair) + deep + back * b, deep)
+        return high * pair + low
 
     def near_peer(step):
-        other = lax.rem(near + step, near_n)
+        other = near_shift(step)
         return other, {"kv": far * near_n + other}
 
     def far_peer(step):
@@ -131,7 +145,7 @@
     def sum_near(ch):
         total = near_out[ch][near].astype(f32)
         for step in range(1, near_n):
-            origin = lax.rem(near + near_n - step, near_n)
+            origin = near_shift(step, -1)
             arrived(
                 near_out[ch].at[origin],
                 near_in[ch].at[origin],
@@ -194,7 +208,7 @@
 
     def gathered(ch):
         for step in range(1, near_n):
-            origin = lax.rem(near + near_n - step, near_n)
+            origin = near_shift(step, -1)
             arrived(
                 ag_near[ch].at[origin],
                 ag_near[ch].at[origin],
@@ -210,25 +224,45 @@
         arrived(swap_out.at[use], swap_in.at[use], ws_sem.at[use], wr_sem.at[use], {"tp": 1 - tp})
         return swap_out[use].astype(f32) + swap_in[use].astype(f32)
 
-    mix_gain = params[:, :width]
-    ffn_gain = params[:, width : 2 * width]
-    head_gain = params[:, 2 * width : 2 * width + val_dim]
-    decay_bias = params[:, 2 * width + val_dim :]
-
-    token_f32 = jnp.dot(perm[...], tokens[...], preferred_element_type=f32)
-    mix_in = (token_f32 * mix_gain).astype(bf16)
-    attn_channels = ((0, h_query, 0), (1, h_decay, 1), (2, h_key, 2), (3, h_value, 3), (4, h_gate, 4))
-    for ch, weight, load in attn_channels:
-        loads[load].wait()
-        put_near(ch, 0, jnp.dot(mix_in, weight[...], preferred_element_type=f32))
+    def gain(ref):
+        return ref[...].astype(f32).reshape(1, -1)
+
+    row_at = lax.broadcasted_iota(jnp.int32, (rows, rows), 0)
+    col_at = lax.broadcasted_iota(jnp.int32, (rows, rows), 1)
+    perm = jnp.zeros((rows, rows), f32)
+    unperm = jnp.zeros((rows, rows), f32)
+    for slot, origin in enumerate(cfg["order"]):
+        perm = jnp.where((row_at == slot) & (col_at == origin), 1.0, perm)
+        unperm = jnp.where((col_at == slot) & (row_at == origin), 1.0, unperm)
+    loads[0].wait()
+    loads[1].wait()
+    token_f32 = jnp.dot(perm.astype(bf16), tokens[...], preferred_element_type=f32)
+    mix_in = (token_f32 * gain(mix_ref)).astype(bf16)
+    first = {}
+    squares = halves(jnp.sum(token_f32 * token_f32, axis=1, keepdims=True))
+    weight_at = {"query": 2, "decay": 3, "key": 4, "value": 6, "gate": 7}
+    for ch, names in enumerate(ATTN_CHANNELS):
+        at = 0
+        for name in names:
+            weight = held[weight_at[name]]
+            loads[weight_at[name]].wait()
+            put_near(ch, at, jnp.dot(mix_in, weight[...], preferred_element_type=f32))
+            first[name] = (ch, at, at + weight.shape[1])
+            at += weight.shape[1]
         if ch == 0:
-            squares = jnp.sum(token_f32 * token_f32, axis=1, keepdims=True)
-            put_near(0, weight.shape[1], halves(squares))
+            put_near(0, at, squares)
+            squares_at = at
             pl.semaphore_wait(barrier, near_n + far_n - 1)
         start_near(ch)
-    key_cols = heads * key_dim
-    for ch in range(5):
-        to_far(ch, key_cols if ch == 0 else None)
+    for ch in range(len(ATTN_CHANNELS)):
+        to_far(ch, squares_at if ch == 0 else None)
+    totals = {}
+
+    def projected(name):
+        ch, low, high = first[name]
+        if ch not in totals:
+            totals[ch] = sum_far(ch)
+        return totals[ch][:, low:high]
 
     def by_head(target, wide, value):
         for row in range(own):
@@ -236,90 +270,110 @@
                 slot = row * heads + head
                 target[slot : slot + 1, :] = value[row : row + 1, head * wide : (head + 1) * wide]
 
-    total = sum_far(0)
-    mix_rms = lax.rsqrt(joined(total[:, key_cols:]) / model_width + epsilon)
-    by_head(q8, key_dim, total[:, :key_cols] * mix_rms * key_dim ** (-0.5))
-    by_head(d8, key_dim, sum_far(1) * mix_rms + decay_bias)
+    loads[5].wait()
+    totals[0] = sum_far(0)
+    mix_rms = lax.rsqrt(joined(totals[0][:, squares_at:]) / model_width + epsilon)
+    by_head(q8, key_dim, projected("query") * mix_rms * key_dim ** (-0.5))
+    by_head(d8, key_dim, projected("decay") * mix_rms + gain(bias_ref))
     decay_in = d8[...]
     log_decay = (jnp.minimum(decay_in, 0.0) - jnp.log1p(jnp.exp(-jnp.abs(decay_in)))) / 16.0
     decay = jnp.exp(log_decay)
-    dec_out[...] = decay.T
+    decay_cols = decay.T
     scaled = (q8[...] * decay).T
-    loads[5].wait()
+    loads[8].wait()
     for row in range(own):
         for head in range(heads):
             slot = row * heads + head
             a8[slot : slot + 1, :] = jnp.sum(h_state[row, head] * scaled[:, slot : slot + 1], axis=0, keepdims=True)
-    by_head(k8, key_dim, sum_far(2) * mix_rms)
-    key_out[...] = k8[...].T
-    by_head(v8, val_dim, sum_far(3) * mix_rms)
-    val_out[...] = v8[...]
-    by_head(g8, val_dim, sum_far(4) * mix_rms)
+    by_head(k8, key_dim, projected("key") * mix_rms)
+    key_cols_t = k8[...].T
+    by_head(v8, val_dim, projected("value") * mix_rms)
+    by_head(g8, val_dim, projected("gate") * mix_rms)
     attended = a8[...] + jnp.sum(q8[...] * k8[...], axis=1, keepdims=True) * v8[...]
     attended = attended * lax.rsqrt(jnp.sum(attended * attended, axis=1, keepdims=True) / val_dim + epsilon)
     gates = g8[...]
-    a8[...] = attended * head_gain * (gates / (1.0 + jnp.exp(-gates)))
+    loads[9].wait()
+    a8[...] = attended * gain(head_ref) * (gates / (1.0 + jnp.exp(-gates)))
     for row in range(own):
         for head in range(heads):
             slot = row * heads + head
             stage[row : row + 1, head * val_dim : (head + 1) * val_dim] = a8[slot : slot + 1, :]
     ag_far[0][far] = stage[:own, : heads * val_dim].astype(bf16)
     start_gather(0)
+    for row in range(own):
+        for head in range(heads):
+            slot = row * heads + head
+            made[row, head] = (
+                decay_cols[:, slot : slot + 1] * h_state[row, head]
+                + key_cols_t[:, slot : slot + 1] * v8[slot : slot + 1, :]
+            )
+    store = pltpu.make_async_copy(made, new_state, out_sem)
+    store.start()
     pass_gather(0)
-    loads[6].wait()
+    loads[11].wait()
     head_partial = jnp.dot(gathered(0), h_output[...], preferred_element_type=f32)
     residual_mid = (token_f32 + over_groups(0, head_partial)).astype(bf16)
 
     mid_f32 = residual_mid.astype(f32)
-    ffn_in = (mid_f32 * ffn_gain).astype(bf16)
+    loads[10].wait()
+    ffn_in = (mid_f32 * gain(ffn_ref)).astype(bf16)
     bounds = cfg["bounds"]
-    loads[7].wait()
-    loads[8].wait()
+    ff_first = len(ATTN_CHANNELS)
+    loads[12].wait()
+    loads[13].wait()
     for index, (low, high) in enumerate(bounds):
-        ch = 5 + index
+        ch = ff_first + index
         put_near(ch, 0, jnp.dot(ffn_in, h_ffgate[:, low:high], preferred_element_type=f32))
         put_near(ch, high - low, jnp.dot(ffn_in, h_ffup[:, low:high], preferred_element_type=f32))
         if index == 0:
             put_near(ch, 2 * (high - low), halves(jnp.sum(mid_f32 * mid_f32, axis=1, keepdims=True)))
         start_near(ch)
-    loads[9].wait()
+    loads[14].wait()
 
     ffn_rms = None
     down = jnp.zeros((rows, width), f32)
-    for turn in range(len(bounds) + 3):
+    for turn in range(len(bounds) + LAGS[2]):
         if turn < len(bounds):
             low, high = bounds[turn]
-            to_far(5 + turn, 2 * (high - low) if turn == 0 else None)
-        index = turn - 1
+            to_far(ff_first + turn, 2 * (high - low) if turn == 0 else None)
+        index = turn - LAGS[0]
         if 0 <= index < len(bounds):
             wide = bounds[index][1] - bounds[index][0]
-            total = sum_far(5 + index)
+            total = sum_far(ff_first + index)
             if index == 0:
                 ffn_rms = lax.rsqrt(joined(total[:, 2 * wide :]) / model_width + epsilon)
             gate = total[:, :wide] * ffn_rms
             up = total[:, wide : 2 * wide] * ffn_rms
             ag_far[1 + index][far] = (gate / (1.0 + jnp.exp(-gate)) * up).astype(bf16)
             start_gather(1 + index)
-        index = turn - 2
+        index = turn - LAGS[1]
         if 0 <= index < len(bounds):
             pass_gather(1 + index)
-        index = turn - 3
+        index = turn - LAGS[2]
         if 0 <= index < len(bounds):
             low, high = bounds[index]
             down = down + jnp.dot(gathered(1 + index), h_down[low:high, :], preferred_element_type=f32)
     mixed = (mid_f32 + over_groups(1, down)).astype(bf16)
-    mixed_ref[...] = jnp.dot(unperm[...], mixed, preferred_element_type=f32).astype(bf16)
+    mixed_ref[...] = jnp.dot(unperm.astype(bf16), mixed, preferred_element_type=f32).astype(bf16)
     for copy in sent:
         copy.wait_send()
-
-
-def state_kernel(decay, keys, values, state, new_state):
-    heads = pl.num_programs(1)
-    slot = pl.program_id(0) * heads + pl.program_id(1)
-    chosen = lax.broadcasted_iota(jnp.int32, decay.shape, 1) == slot
-    decay_col = jnp.sum(jnp.where(chosen, decay[...], 0.0), axis=1, keepdims=True)
-    key_col = jnp.sum(jnp.where(chosen, keys[...], 0.0), axis=1, keepdims=True)
-    new_state[0, 0] = decay_col * state[0, 0] + key_col * values[pl.ds(slot, 1), :]
+    store.wait()
+
+
+def hand_over(mixed_in, state_in, mixed_out, state_out, mixed_held, state_held, in_sem, out_sem):
+    own, heads = state_in.shape[:2]
+    places = [(row, head) for row in range(own) for head in range(heads)]
+    moves = [(mixed_in, mixed_held, mixed_out)]
+    moves += [(state_in.at[place], state_held.at[place], state_out.at[place]) for place in places]
+    loads = [pltpu.make_async_copy(move[0], move[1], in_sem.at[slot]) for slot, move in enumerate(moves)]
+    stores = [pltpu.make_async_copy(move[1], move[2], out_sem.at[slot]) for slot, move in enumerate(moves)]
+    for load in loads:
+        load.start()
+    for load, store in zip(loads, stores):
+        load.wait()
+        store.start()
+    for store in stores:
+        store.wait()
 
 
 def local_fused(
@@ -347,7 +401,9 @@
     slots = own * heads
     bounds = ff_bounds(w_down.shape[0])
     key_cols, val_cols = heads * key_dim, heads * val_dim
-    rs_widths = [key_cols + 2 * LANES, key_cols, key_cols, val_cols, val_cols]
+    extents = {"query": key_cols, "decay": key_cols, "key": key_cols, "value": val_cols, "gate": val_cols}
+    rs_widths = [sum(extents[name] for name in names) for names in ATTN_CHANNELS]
+    rs_widths[0] += 2 * LANES
     rs_widths += [2 * (high - low) + (2 * LANES if low == 0 else 0) for low, high in bounds]
     ag_widths = [val_cols] + [high - low for low, high in bounds]
     cfg = {
@@ -355,12 +411,10 @@
         "rs_widths": rs_widths,
         "ag_widths": ag_widths,
         "bounds": bounds,
+        "order": np.arange(rows).reshape(far_n, near_n, own).transpose(1, 0, 2).reshape(-1).tolist(),
     }
-    origin = np.arange(rows).reshape(far_n, near_n, own).transpose(1, 0, 2).reshape(-1)
-    order = np.zeros((rows, rows), np.float32)
-    order[np.arange(rows), origin] = 1.0
-    params = jnp.concatenate([mix_gain.astype(f32), ffn_gain.astype(f32), head_gain.astype(f32), decay_bias])[None]
-    held = [w_query, w_decay, w_key, w_value, w_gate, state, w_output, w_ffgate, w_ffup, w_down]
+    held = [tokens, mix_gain, w_query, w_decay, w_key, decay_bias, w_value, w_gate, state]
+    held += [head_gain, ffn_gain, w_output, w_ffgate, w_ffup, w_down]
     scratch = [pltpu.VMEM(array.shape, array.dtype) for array in held]
     scratch += [pltpu.VMEM((near_n, block, wide), bf16) for wide in rs_widths] * 2
     scratch += [pltpu.VMEM((far_n, own, wide), bf16) for wide in rs_widths] * 2
@@ -369,53 +423,39 @@
     scratch += [pltpu.VMEM((block, max(ag_widths)), f32)]
     scratch += [pltpu.VMEM((2, rows, width), bf16)] * 2
     scratch += [pltpu.VMEM((slots, wide), f32) for wide in (key_dim, key_dim, key_dim, val_dim, val_dim, val_dim)]
+    scratch += [pltpu.VMEM(state.shape, f32)]
     dma = pltpu.SemaphoreType.DMA
-    scratch += [dma((len(held),))]
+    scratch += [dma((15,))]
     scratch += [dma((len(rs_widths), near_n))] * 2 + [dma((len(rs_widths), far_n))] * 2
     scratch += [dma((len(ag_widths), far_n))] * 2 + [dma((len(ag_widths), near_n))] * 2
     scratch += [dma((2,))] * 2
+    scratch += [dma]
     vmem = pl.BlockSpec(memory_space=pltpu.VMEM)
-    hbm = pl.BlockSpec(memory_space=pl.ANY)
-    mixed, decay, keys, values = pl.pallas_call(
+    hbm = pl.BlockSpec(memory_space=pltpu.HBM)
+    results = pl.pallas_call(
         functools.partial(layer_kernel, cfg),
-        out_shape=(
-            jax.ShapeDtypeStruct((rows, width), bf16),
-            jax.ShapeDtypeStruct((key_dim, slots), f32),
-            jax.ShapeDtypeStruct((key_dim, slots), f32),
-            jax.ShapeDtypeStruct((slots, val_dim), f32),
-        ),
-        in_specs=[vmem] * 4 + [hbm] * 10,
-        out_specs=(vmem,) * 4,
+        out_shape=(jax.ShapeDtypeStruct((rows, width), bf16), jax.ShapeDtypeStruct(state.shape, f32)),
+        in_specs=[hbm] * len(held),
+        out_specs=(vmem, hbm),
         scratch_shapes=scratch,
         compiler_params=pltpu.CompilerParams(
-            collective_id=0, has_side_effects=True, vmem_limit_bytes=48 * 1024 * 1024
+            collective_id=0, has_side_effects=True, vmem_limit_bytes=VMEM_BYTES
         ),
-    )(
-        tokens,
-        params,
-        jnp.asarray(order, bf16),
-        jnp.asarray(order.T, bf16),
-        w_query,
-        w_key,
-        w_value,
-        w_gate,
-        w_decay,
-        w_output,
-        w_ffgate,
-        w_ffup,
-        w_down,
-        state,
-    )
-    whole = pl.BlockSpec((key_dim, slots), lambda row, head: (0, 0))
-    tile = pl.BlockSpec((1, 1, key_dim, val_dim), lambda row, head: (row, head, 0, 0))
-    new_state = pl.pallas_call(
-        state_kernel,
-        grid=(own, heads),
-        out_shape=jax.ShapeDtypeStruct(state.shape, f32),
-        in_specs=[whole, whole, pl.BlockSpec((slots, val_dim), lambda row, head: (0, 0)), tile],
-        out_specs=tile,
-    )(decay, keys, values, state)
-    return (mixed, new_state)
+    )(*held)
+    dma = pltpu.SemaphoreType.DMA
+    return pl.pallas_call(
+        hand_over,
+        out_shape=(jax.ShapeDtypeStruct((rows, width), bf16), jax.ShapeDtypeStruct(state.shape, f32)),
+        in_specs=[hbm] * 2,
+        out_specs=(hbm,) * 2,
+        scratch_shapes=[
+            pltpu.VMEM((rows, width), bf16),
+            pltpu.VMEM(state.shape, f32),
+            dma((1 + slots,)),
+            dma((1 + slots,)),
+        ],
+        compiler_params=pltpu.CompilerParams(vmem_limit_bytes=VMEM_BYTES),
+    )(*results)
 
 
 def local_plain(

time: 73.2 us -> 53.5 us (0.73)
  local copies, waits for them, and re-layouts: 10.7 us -> 0 us
  Pallas kernels: 58.5 us -> 52.5 us
  other arithmetic: 2.69 us -> 0 us
    unnamed x23 -> x0, local copies, waits for them, and re-layouts: 10.7 us -> none
    pallas_call x1, Pallas kernels: 7.12 us -> 3.64 us  [local_fused(): pl.pallas_call(hand_over, out_shape=(jax.ShapeDtypeStruct((rows, width),...]
    pallas_call x1, Pallas kernels: 51.3 us -> 48.9 us  [local_fused(): pl.pallas_call(functools.partial(layer_kernel, cfg), out_shape=(jax.Shape...]
    convert_element_type x3 -> x0, other arithmetic: 2 us -> none  [the longest x1 0.68 us: local_fused(): head_gain.astype(f32)]
where the time goes in v2:
time: 53.5 us; the launch traced here: 53.2 us
  Pallas kernels  52.5 us (98%)
  between operations  0.64 us (1%)
    pallas_call x1, Pallas kernels, local_fused(): pl.pallas_call(functools.partial(layer_kernel, cfg), out_shape=(jax.Shape...  48.9 us
    pallas_call x1, Pallas kernels, local_fused(): pl.pallas_call(hand_over, out_shape=(jax.ShapeDtypeStruct((rows, width),...  3.64 us

profile of v2, /device:TPU:1, one launch (start us, length us, event | category | flops | bytes accessed | tf_op | source)
XLA Modules:
  0.0 53.2 jit_solution(3492220763184383738)
XLA Ops:
  0.6 48.9 %shard_map.158 = (bf16[32,256]{1,0:T(8,128)(2,1)}, f32[2,4,256,512]{3,2,1,0:T(8,128)}) custom-call(bf16[32,256]{1,0:T(8,128)(2,1)} %refs_0_.1, bf16[256]{0:T(256)(128)(2,1)} %refs_1_.1, bf16[256,1024]{1,0:T(8,128)(2,1)} %refs_2_.1, bf16[256,1024]{1,0:T(8,128)(2,1)} %refs_3_.1, bf16[256,1024]{1,0:T(8,128)(2,1)} %refs_4_.1, f32[1024]{0:T(1024)} %refs_5_.1, ...), custom_call_target="tpu_custom_call" | custom-call | tf_op jit(solution)/shard_map/pallas_call | solution.py:435
  49.5 3.6 %shard_map.159 = (bf16[32,256]{1,0:T(8,128)(2,1)}, f32[2,4,256,512]{3,2,1,0:T(8,128)}) custom-call(bf16[32,256]{1,0:T(8,128)(2,1)} %get-tuple-element.4.mixed_in, f32[2,4,256,512]{3,2,1,0:T(8,128)} %get-tuple-element.5.state_in), custom_call_target="tpu_custom_call" | custom-call | tf_op jit(solution)/shard_map/pallas_call | solution.py:446
